TPU v7x, 32 devices: a whole 2x2x4 slice. The times are simulated.
32 devices in a mesh: grp: 2 (over y), ep: 4 (over z), tp: 4 (over x, core).
Axes of the slice: x: 2, y: 2, z: 4, core: 2. Of those that a mesh axis runs over, the one named last changes fastest.
Arguments:
- queries: bfloat16 [2048, 2048], P(('grp', 'ep'), 'tp'), parts along dimension 0, may hold values from -8 to 8
- keys: bfloat16 [2048, 512], P(('grp', 'ep')), parts along dimension 0, may hold values from -8 to 8
- values: bfloat16 [2048, 512], P(('grp', 'ep')), parts along dimension 0, may hold values from -6 to 6
- q_gain: float32 [128], replicated, may hold values from 0.6 to 5.8
- k_gain: float32 [128], replicated, may hold values from 0.6 to 5.8
- w_out: bfloat16 [2048, 2048], P(None, 'tp'), may hold values from -0.125 to 0.125
- moe_rows: bfloat16 [1536, 2048], P(('grp', 'ep')), parts along dimension 0, may hold values from -6 to 6
- routes: int32 [1536, 2], P(('grp', 'ep')), parts along dimension 0, may hold values from 0 to 3, all different within a row; in each aligned block of 192 rows (0 to 191, 192 to 383, ...) at most 144 rows name the same one
- group_gate: float32 [1536], P(('grp', 'ep')), parts along dimension 0, may hold values from 0.25 to 1
- expert_logits: float32 [1536, 2], P(('grp', 'ep')), parts along dimension 0, may hold values from -6 to 6
- moe_gain: float32 [2048], replicated, may hold values from 0.1 to 1.9
- w_gate: bfloat16 [4, 2048, 2048], P('ep', None, 'tp'), may hold values from -0.125 to 0.125
- w_up: bfloat16 [4, 2048, 2048], P('ep', None, 'tp'), may hold values from -0.125 to 0.125
- w_down: bfloat16 [4, 2048, 2048], P('ep', 'tp'), may hold values from -0.125 to 0.125
Outputs:
- attn_out: bfloat16 [2048, 2048], P(('grp', 'ep'), 'tp'), parts along dimension 0
- moe_out: bfloat16 [1536, 2048], P(('grp', 'ep'), 'tp'), parts along dimension 0
There are 2 independent parts, one for each index of `grp`. A program takes and returns all parts, laid end to end along the dimension named above; an argument that names none is the same for every part. Nothing has to cross between parts.
Inputs may be any that keep to these rules, and one draw needn't show every extreme that they name: `routes`: each row names 2 different experts; within the rows of one index of ep no expert is named more than 144 times, a bound that some block reaches.
All inputs are finite; a program needn't handle non-finite values.
Results may differ from a plain program's by a relative error of at most 0.019.
The roundings to bfloat16 on the way count: a program that leaves them out, or rounds other values in their place, can miss the bound.
Values may be sent and summed in bfloat16 or wider, within the bound.
A program may use at most 64 MiB of HBM per device.

v0:
```python
import jax
import jax.numpy as jnp
from jax import lax
from jax.sharding import PartitionSpec as P

HEADS = 16
KV_HEADS = 4
HEAD_DIM = 128
GRID_W = 64
TOPK = 2


def head_norm(x, gain):
    wide = x.astype(jnp.float32)
    return wide * lax.rsqrt(jnp.mean(wide * wide, axis=-1, keepdims=True) + 1e-06) * gain


def rotate(x, first):
    count = x.shape[0]
    pos = first + jnp.arange(count, dtype=jnp.int32)
    row = (pos // GRID_W).astype(jnp.float32)
    col = (pos % GRID_W).astype(jnp.float32)
    nfreq = HEAD_DIM // 4
    inverse = 10000.0 ** (-jnp.arange(nfreq, dtype=jnp.float32) / nfreq)
    angle = jnp.concatenate(
        [
            row[:, None] * inverse,
            row[:, None] * inverse,
            col[:, None] * inverse,
            col[:, None] * inverse,
        ],
        axis=1,
    )
    parts = x.reshape(x.shape[:-1] + (2, 2, nfreq))
    turned = jnp.stack([-parts[..., 1, :], parts[..., 0, :]], axis=-2).reshape(x.shape)
    return x * jnp.cos(angle)[:, None, :] + turned * jnp.sin(angle)[:, None, :]


def per_device(
    queries,
    keys,
    values,
    q_gain,
    k_gain,
    w_out,
    moe_rows,
    routes,
    group_gate,
    expert_logits,
    moe_gain,
    w_gate,
    w_up,
    w_down,
):
    rows = queries.shape[0]
    heads_dev = queries.shape[1] // HEAD_DIM
    group = HEADS // KV_HEADS
    kv_dev = max(1, heads_dev // group)
    per_kv = heads_dev // kv_dev
    first_kv = lax.axis_index("tp") * heads_dev // group
    first_row = lax.axis_index("ep") * rows
    k_mine = lax.dynamic_slice_in_dim(keys, first_kv * HEAD_DIM, kv_dev * HEAD_DIM, 1)
    v_mine = lax.dynamic_slice_in_dim(values, first_kv * HEAD_DIM, kv_dev * HEAD_DIM, 1)
    k_rot = rotate(head_norm(k_mine.reshape(rows, kv_dev, HEAD_DIM), k_gain), first_row)
    k_rot = k_rot.astype(jnp.bfloat16).reshape(rows, kv_dev * HEAD_DIM)
    q_rot = rotate(head_norm(queries.reshape(rows, heads_dev, HEAD_DIM), q_gain), first_row)
    q_rot = q_rot.astype(jnp.bfloat16).reshape(rows, kv_dev, per_kv, HEAD_DIM)
    scale = HEAD_DIM ** (-0.5)
    top = jnp.full((rows, kv_dev, per_kv), -jnp.inf, jnp.float32)
    total = jnp.zeros((rows, kv_dev, per_kv), jnp.float32)
    acc = jnp.zeros((rows, kv_dev, per_kv, HEAD_DIM), jnp.float32)
    k_piece = lax.all_gather(k_rot, "ep", axis=0, tiled=True)
    v_piece = lax.all_gather(v_mine, "ep", axis=0, tiled=True)
    count = k_piece.shape[0]
    key_rows = k_piece.reshape(count, kv_dev, HEAD_DIM)
    value_rows = v_piece.reshape(count, kv_dev, HEAD_DIM)
    scores = (
        jnp.einsum("qkgd,nkd->qkgn", q_rot, key_rows, preferred_element_type=jnp.float32) * scale
    )
    new_top = jnp.max(scores, axis=-1)
    shrink = jnp.exp(top - new_top)
    expo = jnp.exp(scores - new_top[..., None])
    total = total * shrink + jnp.sum(expo, axis=-1)
    acc = acc * shrink[..., None] + jnp.einsum(
        "qkgn,nkd->qkgd", expo.astype(jnp.bfloat16), value_rows, preferred_element_type=jnp.float32
    )
    top, total, acc = (new_top, total, acc)
    mixed = (acc / total[..., None]).astype(jnp.bfloat16).reshape(rows, heads_dev * HEAD_DIM)
    attn_out = jnp.dot(
        lax.all_gather(mixed, "tp", axis=1, tiled=True), w_out, preferred_element_type=jnp.float32
    ).astype(jnp.bfloat16)
    count = moe_rows.shape[0]
    width = moe_rows.shape[1]
    peers = lax.axis_size("ep")
    capacity = 3 * count // peers
    wide = moe_rows.astype(jnp.float32)
    normed = (
        wide * lax.rsqrt(jnp.mean(wide * wide, axis=-1, keepdims=True) + 1e-06) * moe_gain
    ).astype(jnp.bfloat16)
    chosen = routes.reshape(-1)
    onehot = (chosen[:, None] == jnp.arange(peers, dtype=jnp.int32)[None, :]).astype(jnp.int32)
    rank = jnp.sum((jnp.cumsum(onehot, axis=0) - onehot) * onehot, axis=1)
    slots = chosen * capacity + rank
    owner = jnp.arange(count * TOPK, dtype=jnp.int32) // TOPK
    source = jnp.zeros((peers * capacity,), jnp.int32).at[slots].set(owner)
    used = jnp.zeros((peers * capacity,), jnp.bool_).at[slots].set(True)
    outgoing = jnp.where(used[:, None], normed[source], jnp.zeros((), jnp.bfloat16)).reshape(
        peers, capacity, width
    )
    part_cols = width // lax.axis_size("tp")
    mine = lax.dynamic_slice_in_dim(outgoing, lax.axis_index("tp") * part_cols, part_cols, 2)
    arrived = lax.all_gather(
        lax.all_to_all(mine, "ep", split_axis=0, concat_axis=0, tiled=True),
        "tp",
        axis=2,
        tiled=True,
    )
    first_dim, second_dim, cols = arrived.shape
    flat = arrived.reshape(first_dim * second_dim, cols)
    gate = jnp.dot(flat, w_gate[0], preferred_element_type=jnp.float32)
    up = jnp.dot(flat, w_up[0], preferred_element_type=jnp.float32)
    hidden = (jax.nn.silu(gate) * up).astype(jnp.bfloat16)
    result = jnp.dot(hidden, w_down[0], preferred_element_type=jnp.float32).astype(jnp.bfloat16)
    partial_value = result.reshape(first_dim, second_dim, cols)
    summed = (
        lax.psum_scatter(partial_value, "tp", scatter_dimension=2, tiled=True)
        .astype(jnp.float32)
        .astype(jnp.bfloat16)
    )
    back = lax.all_to_all(summed, "ep", split_axis=0, concat_axis=0, tiled=True)
    back = back.reshape(peers * capacity, back.shape[2])
    picked = back[slots].astype(jnp.float32).reshape(count, TOPK, back.shape[1])
    weights = group_gate[:, None] * jax.nn.softmax(expert_logits, axis=-1)
    moe_out = jnp.sum(weights[:, :, None] * picked, axis=1).astype(jnp.bfloat16)
    return (attn_out, moe_out)


def solution(mesh):
    placed = (
        P(("grp", "ep"), "tp"),
        P(("grp", "ep"), None),
        P(("grp", "ep"), None),
        P(),
        P(),
        P(None, "tp"),
        P(("grp", "ep"), None),
        P(("grp", "ep"), None),
        P(("grp", "ep")),
        P(("grp", "ep"), None),
        P(),
        P("ep", None, "tp"),
        P("ep", None, "tp"),
        P("ep", "tp", None),
    )
    return jax.shard_map(
        per_device,
        mesh=mesh,
        in_specs=placed,
        out_specs=(P(("grp", "ep"), "tp"), P(("grp", "ep"), "tp")),
        check_vma=False,
    )
```

profile of v0, /device:TPU:0, one launch (start us, length us, event | category | flops | bytes accessed | tf_op | source)
XLA Modules:
  0.0 148.1 jit_solution(11262557061539180350)
XLA Ops:
  7.2 0.9 copy.30
  8.2 0.1 eq.32
  8.3 0.1 eq.28
  8.5 0.7 broadcast_multiply_fusion.2
  9.2 1.2 reduce-window.6
  10.4 0.2 slice_reduce_fusion
  10.6 0.2 reduce-window.9
  10.8 0.1 add_bitcast_fusion
  10.8 0.1 copy.29
  11.0 0.1 mul.316
  11.2 2.9 %scatter_custom_fusion.1 = s32[576]{0:T(1024)S(1)} fusion(s32[384]{0:T(512)S(1)} %fusion.58, s32[384]{0:T(512)S(1)} %add_select_fusion, s32[]{:T(128)} %constant.95.clone.1), kind=kCustom, calls=%fused_computation.81 | custom fusion | bytes 2308 | tf_op jit(solution)/shard_map/scatter | solution.py:105
  14.1 1.4 fusion.13
  15.5 2.0 %scatter_custom_fusion = pred[576]{0:T(1024)(128)(4,1)S(1)} fusion(s32[384]{0:T(512)S(1)} %fusion.58, pred[384]{0:T(512)(128)(4,1)S(1)} %broadcast.278, pred[]{:T(512)} %constant.115.clone.1), kind=kCustom, calls=%fused_computation.86 | custom fusion | bytes 577 | tf_op jit(solution)/shard_map/scatter | solution.py:106
  17.5 0.1 broadcast_in_dim.24
  17.6 1.4 fusion.15
  19.0 4.0 %gather_fusion = bf16[576,2048]{1,0:T(8,128)(2,1)} fusion(bf16[192,2048]{1,0:T(8,128)(2,1)S(1)} %fusion.15, s32[1024]{0:T(1024)S(1)} %pad_clamp_fusion.1), kind=kCustom, calls=%fused_computation | custom fusion | bytes 4720896 | tf_op jit(solution)/shard_map/gather | solution.py:107
  23.0 1.3 dynamic-slice_select_fusion
  24.3 22.1 %all_to_all.10 = bf16[4,144,512]{2,1,0:T(8,128)(2,1)} all-to-all(bf16[4,144,512]{2,1,0:T(8,128)(2,1)S(1)} %dynamic-slice_select_fusion), channel_id=1, replica_groups=mesh['grp'=2,'ep'=4,'tp'=4] {'ep'}, dimensions={0} | all-to-all | bytes 1179648 | tf_op jit(solution)/shard_map/all_to_all | solution.py:113
  46.5 23.3 %all-gather.5.cloned.1.call-done = bf16[4,144,2048]{2,1,0:T(8,128)(2,1)} async-done(((bf16[4,144,512]{2,1,0:T(8,128)(2,1)}), bf16[4,144,2048]{2,1,0:T(8,128)(2,1)}) %all-gather.5.cloned.1.call-update) | async-done | bytes 2359312 | tf_op jit(solution)/shard_map/all_gather | solution.py:112
  69.7 4.7 %fusion.9 = f32[576,512]{1,0:T(8,128)} fusion(bf16[576,2048]{1,0:T(8,128)(2,1)} %bitcast.131, bf16[1,2048,512]{2,1,0:T(8,128)(2,1)} %param.25), kind=kOutput, calls=%fused_computation.15 | convolution fusion | flops 1207959552 | bytes 5636096 | tf_op jit(solution)/shard_map/dot_general | solution.py:120
  74.5 6.7 %convolution_convert_fusion = bf16[576,2048]{1,0:T(8,128)(2,1)} fusion(bf16[1,512,2048]{2,1,0:T(8,128)(2,1)S(1)} %copy-done, bf16[576,2048]{1,0:T(8,128)(2,1)} %bitcast.132, bf16[1,2048,512]{2,1,0:T(8,128)(2,1)} %param.26, f32[576,512]{1,0:T(8,128)} %fusion.9), kind=kOutput, calls=%fused_computation.9 | convolution fusion | flops 2418868224 | bytes 10092544 | tf_op jit(solution)/shard_map/dot_general | solution.py:123
  81.3 0.8 copy-done.2
  82.1 0.1 fusion.43
  82.3 0.1 fusion.44
  82.4 0.1 copy.20
  82.5 0.1 copy.21
  82.7 0.1 broadcast_multiply_fusion.1
  82.8 0.6 add_convert_fusion
  83.4 0.1 copy.23
  83.5 0.1 copy.24
  83.6 0.1 copy.22
  83.8 0.1 mul.300
  83.8 0.8 constant_dynamic-slice_fusion
  84.7 0.1 copy.34
  84.9 0.1 multiply_multiply_fusion
  85.1 0.2 fusion.38
  85.3 13.9 %all_gather.12 = bf16[1024,128]{1,0:T(8,128)(2,1)S(1)} all-gather(bf16[256,128]{1,0:T(8,128)(2,1)S(1)} %get-tuple-element.2), channel_id=1, replica_groups=mesh['grp'=2,'ep'=4,'tp'=4] {'ep'}, dimensions={0}, use_global_device_ids=true | all-gather | bytes 327680 | tf_op jit(solution)/shard_map/all_gather | solution.py:72
  99.2 14.7 %all_gather.13 = bf16[1024,128]{0,1:T(8,128)(2,1)S(1)} all-gather(bf16[256,128]{0,1:T(8,128)(2,1)S(1)} %copy.34), channel_id=1, replica_groups=mesh['grp'=2,'ep'=4,'tp'=4] {'ep'}, dimensions={0}, use_global_device_ids=true | all-gather | bytes 327680 | tf_op jit(solution)/shard_map/all_gather | solution.py:73
  113.9 0.7 bitcast_reduce_fusion
  114.6 0.7 fusion.1
  115.4 1.6 %fusion.31 = bf16[1,128,256,4]{2,1,3,0:T(8,128)(2,1)} fusion(f32[1024,256,4]{1,0,2:T(8,128)S(1)} %get-tuple-element.14, f32[256,4]{0,1:T(4,128)S(1)} %get-tuple-element.13, bf16[1024,128]{0,1:T(8,128)(2,1)S(1)} %all_gather.13, f32[256,4]{0,1:T(4,128)S(1)} %get-tuple-element.10, f32[256,4]{0,1:T(4,128)S(1)} %get-tuple-element.9), kind=kOutput, calls=%fused_computation.30 | convolution fusion | flops 271974400 | bytes 4730880 | tf_op jit(solution)/shard_map/qkgn,nkd->qkgd/dot_general | solution.py:84
  117.0 4.8 %all-to-all-start.1 = ((bf16[4,144,512]{2,1,0:T(8,128)(2,1)}), bf16[4,144,512]{2,1,0:T(8,128)(2,1)S(1)}, u32[]{:S(2)}, u32[]{:S(2)}) async-start(bf16[4,144,512]{2,1,0:T(8,128)(2,1)} %reduce-scatter.2.cloned.1.call-done), calls=%async_computation.2 | async-start | bytes 1179648 | tf_op jit(solution)/shard_map/all_to_all | solution.py:130
  121.8 0.1 copy.28
  122.0 12.0 %all-gather.3.cloned.1.call-done = bf16[256,2048]{0,1:T(8,128)(2,1)} async-done(((bf16[256,512]{0,1:T(8,128)(2,1)}), bf16[256,2048]{0,1:T(8,128)(2,1)}) %all-gather.3.cloned.1.call-update) | async-done | bytes 1048592 | tf_op jit(solution)/shard_map/all_gather | solution.py:90
  134.0 3.3 %convolution_convert_fusion.1 = bf16[256,512]{1,0:T(8,128)(2,1)} fusion(bf16[256,2048]{0,1:T(8,128)(2,1)} %all-gather.3.cloned.1.call-done, bf16[2048,512]{1,0:T(8,128)(2,1)} %param.19), kind=kOutput, calls=%fused_computation.28 | convolution fusion | flops 537001984 | bytes 3407872 | tf_op jit(solution)/shard_map/dot_general | solution.py:89
  137.3 2.1 %gather_fusion.1 = bf16[384,512]{1,0:T(8,128)(2,1)S(1)} fusion(bf16[576,512]{1,0:T(8,128)(2,1)S(1)} %bitcast.122, s32[1024]{0:T(1024)S(1)} %pad_clamp_fusion), kind=kCustom, calls=%fused_computation.1 | custom fusion | bytes 787968 | tf_op jit(solution)/shard_map/gather | solution.py:132
  139.4 0.5 reshape.352
  139.9 1.7 %multiply_reduce_fusion = bf16[192,512]{1,0:T(8,128)(2,1)} fusion(f32[192,2,512]{2,1,0:T(2,128)S(1)} %reshape.352, f32[192,2]{1,0:T(8,128)S(1)} %copy.28), kind=kLoop, calls=%fused_computation.31 | loop fusion | flops 294912 | bytes 984576 | tf_op jit(solution)/shard_map/reduce_sum | solution.py:134
  (44 shorter events, 0.6 us)
Async XLA Ops:
  7.2 67.3 %copy-start = (bf16[1,512,2048]{2,1,0:T(8,128)(2,1)S(1)}, bf16[1,512,2048]{2,1,0:T(8,128)(2,1)}, u32[]{:S(2)}) copy-start(bf16[1,512,2048]{2,1,0:T(8,128)(2,1)} %param.27) | copy-start | bytes 6291460
  7.2 62.6 %all-gather.5.cloned.1.call-start = ((), (), s32[]{:S(2)}) async-start(), calls=%async_computation.4 | async-start | bytes 2949120 | tf_op jit(solution)/shard_map/all_gather | solution.py:112
  46.4 70.6 %reduce-scatter.2.cloned.1.call-start = ((), (), s32[]{:S(2)}) async-start(), calls=%async_computation.5 | async-start | bytes 2949120 | tf_op jit(solution)/shard_map/reduce_scatter | solution.py:126
  81.2 0.9 copy-start.2
  81.2 1.1 copy-start.4
  81.2 2.4 %copy-start.1 = (bf16[256,512]{1,0:T(8,128)(2,1)S(1)}, bf16[256,512]{1,0:T(8,128)(2,1)}, u32[]{:S(2)}) copy-start(bf16[256,512]{1,0:T(8,128)(2,1)} %param.14) | copy-start | bytes 786436
  81.2 2.5 %copy-start.5 = (f32[128]{0:T(128)S(1)}, f32[128]{0:T(128)}, u32[]{:S(2)}) copy-start(f32[128]{0:T(128)} %param.17) | copy-start | bytes 1540
  81.2 52.8 %all-gather.3.cloned.1.call-start = ((), (), s32[]{:S(2)}) async-start(), calls=%async_computation.3 | async-start | bytes 1310720 | tf_op jit(solution)/shard_map/all_gather | solution.py:90
  115.3 6.4 %copy-start.3 = (f32[192,2]{0,1:T(2,128)S(1)}, f32[192,2]{0,1:T(2,128)}, u32[]{:S(2)}) copy-start(f32[192,2]{0,1:T(2,128)} %param.23) | copy-start | bytes 4612
  115.3 6.5 %copy-start.6 = (f32[192]{0:T(256)S(1)}, f32[192]{0:T(256)}, u32[]{:S(2)}) copy-start(f32[192]{0:T(256)} %param.22) | copy-start | bytes 2308
  117.0 20.3 %all-to-all-start.1 = ((bf16[4,144,512]{2,1,0:T(8,128)(2,1)}), bf16[4,144,512]{2,1,0:T(8,128)(2,1)S(1)}, u32[]{:S(2)}, u32[]{:S(2)}) async-start(bf16[4,144,512]{2,1,0:T(8,128)(2,1)} %reduce-scatter.2.cloned.1.call-done), calls=%async_computation.2 | async-start | bytes 1179648 | tf_op jit(solution)/shard_map/all_to_all | solution.py:130
Sparse Core Ops, SparseCore 0:
  46.5 23.1 all-gather.4
  81.3 32.7 reduce-scatter.1
  117.1 16.8 all-gather.2
where the time goes:
time: 149 us; the launch traced here: 148 us
  blocking collectives  50.8 us (34%)
  waiting for transfers between devices  35.3 us (24%)
  matrix products  17.1 us (11%)
  local copies, waits for them, and re-layouts  15.8 us (11%)
  between operations  14.1 us (9%)
  other arithmetic  10.1 us (7%)
  starting transfers between devices  4.88 us (3%)
    all_gather x1, waiting for transfers between devices, per_device(): lax.all_gather(lax.all_to_all(mine, 'ep', split_axis=0, concat_axis=0, ti...  23.3 us
    all_to_all x1, blocking collectives, per_device(): lax.all_to_all(mine, 'ep', split_axis=0, concat_axis=0, tiled=True)  22.1 us
    all_gather x1, blocking collectives, per_device(): v_piece = lax.all_gather(v_mine, 'ep', axis=0, tiled=True)  14.7 us
    all_gather x1, blocking collectives, per_device(): k_piece = lax.all_gather(k_rot, 'ep', axis=0, tiled=True)  13.9 us
    all_gather x1, waiting for transfers between devices, per_device(): lax.all_gather(mixed, 'tp', axis=1, tiled=True)  12 us
    dot_general x1, matrix products, per_device(): jnp.dot(hidden, w_down[0], preferred_element_type=jnp.float32)  6.71 us
    all_to_all x1, starting transfers between devices, per_device(): back = lax.all_to_all(summed, 'ep', split_axis=0, concat_axis=0, tiled=True)  4.76 us
    dot_general x1, matrix products, per_device(): gate = jnp.dot(flat, w_gate[0], preferred_element_type=jnp.float32)  4.74 us
  transfers between devices with their start and end apart: 4, of which 2 were waited for; matrix products, arithmetic and copies ran while one was open for 6% of the time, Pallas kernels for 0%

commit v1 on v0

--- a/solution.py
+++ b/solution.py
@@ -8,6 +8,16 @@
 HEAD_DIM = 128
 GRID_W = 64
 TOPK = 2
+
+
+def pass_along(value, mesh_axis, d):
+    size = lax.axis_size(mesh_axis)
+    moving, pieces = (value, [value])
+    for _ in range(size - 1):
+        moving = lax.ppermute(moving, mesh_axis, [(i, (i + 1) % size) for i in range(size)])
+        pieces.insert(0, moving)
+    line = jnp.concatenate(pieces, axis=d)
+    return jnp.roll(line, (lax.axis_index(mesh_axis) + 1) * value.shape[d], axis=d)
 
 
 def head_norm(x, gain):
@@ -69,7 +79,7 @@
     top = jnp.full((rows, kv_dev, per_kv), -jnp.inf, jnp.float32)
     total = jnp.zeros((rows, kv_dev, per_kv), jnp.float32)
     acc = jnp.zeros((rows, kv_dev, per_kv, HEAD_DIM), jnp.float32)
-    k_piece = lax.all_gather(k_rot, "ep", axis=0, tiled=True)
+    k_piece = pass_along(k_rot, "ep", 0)
     v_piece = lax.all_gather(v_mine, "ep", axis=0, tiled=True)
     count = k_piece.shape[0]
     key_rows = k_piece.reshape(count, kv_dev, HEAD_DIM)

time: 149 us -> 148 us (level)
  blocking collectives: 50.8 us -> 36.3 us
  waiting for transfers between devices: 35.3 us -> 47.5 us
    all_gather x1 -> x0, blocking collectives: 13.9 us -> none  [per_device(): k_piece = lax.all_gather(k_rot, 'ep', axis=0, tiled=True)]
    ppermute x0 -> x3, waiting for transfers between devices: none -> 8.75 us  [pass_along(): lax.ppermute(moving, mesh_axis, [(i, (i + 1) % size) for i in range(size)])]
    all_gather x1, waiting for transfers between devices: 12 us -> 14.1 us  [per_device(): lax.all_gather(mixed, 'tp', axis=1, tiled=True)]
    reduce_scatter x1, waiting for transfers between devices: 0.02 us -> 1.57 us  [per_device(): lax.psum_scatter(partial_value, 'tp', scatter_dimension=2, tiled=True)]
    ppermute x0 -> x3, starting transfers between devices: none -> 1.54 us  [pass_along(): lax.ppermute(moving, mesh_axis, [(i, (i + 1) % size) for i in range(size)])]
  transfers between devices with their start and end apart: 4 -> 7, of which waited for: 2 -> 5; matrix products, arithmetic and copies ran while one was open for 6% -> 7% of each run, Pallas kernels for 0% -> 0%
where the time goes in v1:
time: 148 us; the launch traced here: 147 us
  waiting for transfers between devices  47.5 us (32%)
  blocking collectives  36.3 us (25%)
  matrix products  17.1 us (12%)
  local copies, waits for them, and re-layouts  15.6 us (11%)
  between operations  14.2 us (10%)
  other arithmetic  10.2 us (7%)
  starting transfers between devices  6.26 us (4%)
    all_gather x1, waiting for transfers between devices, per_device(): lax.all_gather(lax.all_to_all(mine, 'ep', split_axis=0, concat_axis=0, ti...  23.1 us
    all_to_all x1, blocking collectives, per_device(): lax.all_to_all(mine, 'ep', split_axis=0, concat_axis=0, tiled=True)  22.1 us
    all_gather x1, blocking collectives, per_device(): v_piece = lax.all_gather(v_mine, 'ep', axis=0, tiled=True)  14.2 us
    all_gather x1, waiting for transfers between devices, per_device(): lax.all_gather(mixed, 'tp', axis=1, tiled=True)  14.1 us
    ppermute x3, waiting for transfers between devices, pass_along(): lax.ppermute(moving, mesh_axis, [(i, (i + 1) % size) for i in range(size)])  8.75 us
    dot_general x1, matrix products, per_device(): jnp.dot(hidden, w_down[0], preferred_element_type=jnp.float32)  6.71 us
    dot_general x1, matrix products, per_device(): gate = jnp.dot(flat, w_gate[0], preferred_element_type=jnp.float32)  4.74 us
    all_to_all x1, starting transfers between devices, per_device(): back = lax.all_to_all(summed, 'ep', split_axis=0, concat_axis=0, tiled=True)  4.6 us
  transfers between devices with their start and end apart: 7, of which 5 were waited for; matrix products, arithmetic and copies ran while one was open for 7% of the time, Pallas kernels for 0%

profile of v1, /device:TPU:0, one launch (start us, length us, event | category | flops | bytes accessed | tf_op | source)
XLA Modules:
  0.0 147.2 jit_solution(12162952591111411645)
XLA Ops:
  7.2 0.9 copy.30
  8.2 0.1 eq.35
  8.3 0.1 eq.31
  8.5 0.7 broadcast_multiply_fusion.2
  9.2 1.2 reduce-window.6
  10.4 0.2 slice_reduce_fusion
  10.6 0.2 reduce-window.9
  10.8 0.1 copy.29
  11.0 0.1 mul.320
  11.2 2.9 %scatter_custom_fusion.1 = s32[576]{0:T(1024)S(1)} fusion(s32[384]{0:T(512)S(1)} %fusion.59, s32[384]{0:T(512)S(1)} %add_select_fusion, s32[]{:T(128)} %constant.114.clone.1), kind=kCustom, calls=%fused_computation.90 | custom fusion | bytes 2308 | tf_op jit(solution)/shard_map/scatter | solution.py:115
  14.1 1.4 fusion.13
  15.5 2.0 %scatter_custom_fusion = pred[576]{0:T(1024)(128)(4,1)S(1)} fusion(s32[384]{0:T(512)S(1)} %fusion.59, pred[384]{0:T(512)(128)(4,1)S(1)} %broadcast.285, pred[]{:T(512)} %constant.137.clone.1), kind=kCustom, calls=%fused_computation.95 | custom fusion | bytes 577 | tf_op jit(solution)/shard_map/scatter | solution.py:116
  17.6 1.4 fusion.15
  19.0 4.0 %gather_fusion = bf16[576,2048]{1,0:T(8,128)(2,1)} fusion(bf16[192,2048]{1,0:T(8,128)(2,1)S(1)} %fusion.15, s32[1024]{0:T(1024)S(1)} %pad_clamp_fusion.1), kind=kCustom, calls=%fused_computation | custom fusion | bytes 4720896 | tf_op jit(solution)/shard_map/gather | solution.py:117
  23.0 1.3 dynamic-slice_select_fusion
  24.3 22.1 %all_to_all.10 = bf16[4,144,512]{2,1,0:T(8,128)(2,1)} all-to-all(bf16[4,144,512]{2,1,0:T(8,128)(2,1)S(1)} %dynamic-slice_select_fusion), channel_id=1, replica_groups=mesh['grp'=2,'ep'=4,'tp'=4] {'ep'}, dimensions={0} | all-to-all | bytes 1179648 | tf_op jit(solution)/shard_map/all_to_all | solution.py:123
  46.6 0.1 fusion.44
  46.7 23.1 %all-gather.5.cloned.1.call-done = bf16[4,144,2048]{2,1,0:T(8,128)(2,1)} async-done(((bf16[4,144,512]{2,1,0:T(8,128)(2,1)}), bf16[4,144,2048]{2,1,0:T(8,128)(2,1)}) %all-gather.5.cloned.1.call-update) | async-done | bytes 2359312 | tf_op jit(solution)/shard_map/all_gather | solution.py:122
  69.8 4.7 %fusion.9 = f32[576,512]{1,0:T(8,128)} fusion(bf16[576,2048]{1,0:T(8,128)(2,1)} %bitcast.131, bf16[1,2048,512]{2,1,0:T(8,128)(2,1)} %param.25), kind=kOutput, calls=%fused_computation.15 | convolution fusion | flops 1207959552 | bytes 5636096 | tf_op jit(solution)/shard_map/dot_general | solution.py:130
  74.5 6.7 %convolution_convert_fusion = bf16[576,2048]{1,0:T(8,128)(2,1)} fusion(bf16[1,512,2048]{2,1,0:T(8,128)(2,1)S(1)} %copy-done, bf16[576,2048]{1,0:T(8,128)(2,1)} %bitcast.132, bf16[1,2048,512]{2,1,0:T(8,128)(2,1)} %param.26, f32[576,512]{1,0:T(8,128)} %fusion.9), kind=kOutput, calls=%fused_computation.9 | convolution fusion | flops 2418868224 | bytes 10092544 | tf_op jit(solution)/shard_map/dot_general | solution.py:133
  81.3 0.6 copy-done.4
  81.9 0.1 fusion.45
  82.0 0.1 copy.20
  82.1 0.1 copy.21
  82.3 0.1 broadcast_multiply_fusion.1
  82.4 0.6 add_convert_fusion
  83.0 1.5 %collective-permute-start = (bf16[256,128]{1,0:T(8,128)(2,1)S(1)}, bf16[256,128]{1,0:T(8,128)(2,1)S(1)}, u32[]{:S(2)}, u32[]{:S(2)}) collective-permute-start(bf16[256,128]{1,0:T(8,128)(2,1)S(1)} %get-tuple-element.2), channel_id=1, source_target_pairs={{0,4},{4,8},{8,12},{12,0},{1,5},{5,9},{9,13},{13,1},{2,6},{6,10},{... | collective-permute-start | bytes 196616 | tf_op jit(solution)/shard_map/ppermute | solution.py:17
  84.5 0.1 copy.23
  84.6 0.1 copy.24
  84.8 0.1 copy.22
  85.1 0.1 multiply_multiply_fusion
  85.2 0.9 constant_dynamic-slice_fusion
  86.1 0.1 copy.34
  86.2 2.9 %collective-permute-done = bf16[256,128]{1,0:T(8,128)(2,1)S(1)} collective-permute-done((bf16[256,128]{1,0:T(8,128)(2,1)S(1)}, bf16[256,128]{1,0:T(8,128)(2,1)S(1)}, u32[]{:S(2)}, u32[]{:S(2)}) %collective-permute-start) | collective-permute-done | bytes 65568 | tf_op jit(solution)/shard_map/ppermute | solution.py:17
  89.2 0.2 fusion.38
  89.3 5.8 %collective-permute-done.1 = bf16[256,128]{1,0:T(8,128)(2,1)S(1)} collective-permute-done((bf16[256,128]{1,0:T(8,128)(2,1)S(1)}, bf16[256,128]{1,0:T(8,128)(2,1)S(1)}, u32[]{:S(2)}, u32[]{:S(2)}) %collective-permute-start.1) | collective-permute-done | bytes 65568 | tf_op jit(solution)/shard_map/ppermute | solution.py:17
  95.2 14.2 %all_gather.9 = bf16[1024,128]{0,1:T(8,128)(2,1)S(1)} all-gather(bf16[256,128]{0,1:T(8,128)(2,1)S(1)} %copy.34), channel_id=1, replica_groups=mesh['grp'=2,'ep'=4,'tp'=4] {'ep'}, dimensions={0}, use_global_device_ids=true | all-gather | bytes 327680 | tf_op jit(solution)/shard_map/all_gather | solution.py:83
  109.5 0.7 bitcast_reduce_fusion
  110.2 0.7 fusion.1
  111.0 1.6 %fusion.31 = bf16[1,128,256,4]{2,1,3,0:T(8,128)(2,1)} fusion(f32[1024,256,4]{1,0,2:T(8,128)S(1)} %get-tuple-element.14, f32[256,4]{0,1:T(4,128)S(1)} %get-tuple-element.13, bf16[1024,128]{0,1:T(8,128)(2,1)S(1)} %all_gather.9, f32[256,4]{0,1:T(4,128)S(1)} %get-tuple-element.10, f32[256,4]{0,1:T(4,128)S(1)} %get-tuple-element.9), kind=kOutput, calls=%fused_computation.30 | convolution fusion | flops 271974400 | bytes 4730880 | tf_op jit(solution)/shard_map/qkgn,nkd->qkgd/dot_general | solution.py:94
  112.6 1.6 %reduce-scatter.2.cloned.1.call-done = bf16[4,144,512]{2,1,0:T(8,128)(2,1)} async-done(((bf16[4,144,2048]{2,1,0:T(8,128)(2,1)}), bf16[4,144,512]{2,1,0:T(8,128)(2,1)}) %reduce-scatter.2.cloned.1.call-update) | async-done | bytes 589840 | tf_op jit(solution)/shard_map/reduce_scatter | solution.py:136
  114.2 4.6 %all-to-all-start.1 = ((bf16[4,144,512]{2,1,0:T(8,128)(2,1)}), bf16[4,144,512]{2,1,0:T(8,128)(2,1)S(1)}, u32[]{:S(2)}, u32[]{:S(2)}) async-start(bf16[4,144,512]{2,1,0:T(8,128)(2,1)} %reduce-scatter.2.cloned.1.call-done), calls=%async_computation.2 | async-start | bytes 1179648 | tf_op jit(solution)/shard_map/all_to_all | solution.py:140
  118.8 0.1 copy.28
  119.0 14.1 %all-gather.3.cloned.1.call-done = bf16[256,2048]{0,1:T(8,128)(2,1)} async-done(((bf16[256,512]{0,1:T(8,128)(2,1)}), bf16[256,2048]{0,1:T(8,128)(2,1)}) %all-gather.3.cloned.1.call-update) | async-done | bytes 1048592 | tf_op jit(solution)/shard_map/all_gather | solution.py:100
  133.0 3.3 %convolution_convert_fusion.1 = bf16[256,512]{1,0:T(8,128)(2,1)} fusion(bf16[256,2048]{0,1:T(8,128)(2,1)} %all-gather.3.cloned.1.call-done, bf16[2048,512]{1,0:T(8,128)(2,1)} %param.19), kind=kOutput, calls=%fused_computation.28 | convolution fusion | flops 537001984 | bytes 3407872 | tf_op jit(solution)/shard_map/dot_general | solution.py:99
  136.4 2.1 %gather_fusion.1 = bf16[384,512]{1,0:T(8,128)(2,1)S(1)} fusion(bf16[576,512]{1,0:T(8,128)(2,1)S(1)} %bitcast.122, s32[1024]{0:T(1024)S(1)} %pad_clamp_fusion), kind=kCustom, calls=%fused_computation.1 | custom fusion | bytes 787968 | tf_op jit(solution)/shard_map/gather | solution.py:142
  138.5 0.5 reshape.352
  139.0 1.7 %multiply_reduce_fusion = bf16[192,512]{1,0:T(8,128)(2,1)} fusion(f32[192,2,512]{2,1,0:T(2,128)S(1)} %reshape.352, f32[192,2]{1,0:T(8,128)S(1)} %copy.28), kind=kLoop, calls=%fused_computation.31 | loop fusion | flops 294912 | bytes 984576 | tf_op jit(solution)/shard_map/reduce_sum | solution.py:144
  (57 shorter events, 0.9 us)
Async XLA Ops:
  7.2 67.4 %copy-start = (bf16[1,512,2048]{2,1,0:T(8,128)(2,1)S(1)}, bf16[1,512,2048]{2,1,0:T(8,128)(2,1)}, u32[]{:S(2)}) copy-start(bf16[1,512,2048]{2,1,0:T(8,128)(2,1)} %param.27) | copy-start | bytes 6291460
  7.2 62.6 %all-gather.5.cloned.1.call-start = ((), (), s32[]{:S(2)}) async-start(), calls=%async_computation.4 | async-start | bytes 2949120 | tf_op jit(solution)/shard_map/all_gather | solution.py:122
  23.0 23.6 %copy-start.2 = (bf16[256,512]{1,0:T(8,128)(2,1)S(1)}, bf16[256,512]{1,0:T(8,128)(2,1)}, u32[]{:S(2)}) copy-start(bf16[256,512]{1,0:T(8,128)(2,1)} %param.15) | copy-start | bytes 786436
  46.5 67.7 %reduce-scatter.2.cloned.1.call-start = ((), (), s32[]{:S(2)}) async-start(), calls=%async_computation.5 | async-start | bytes 2949120 | tf_op jit(solution)/shard_map/reduce_scatter | solution.py:136
  81.2 0.7 copy-start.4
  81.2 3.5 %copy-start.1 = (bf16[256,512]{1,0:T(8,128)(2,1)S(1)}, bf16[256,512]{1,0:T(8,128)(2,1)}, u32[]{:S(2)}) copy-start(bf16[256,512]{1,0:T(8,128)(2,1)} %param.14) | copy-start | bytes 786436
  81.3 3.6 %copy-start.5 = (f32[128]{0:T(128)S(1)}, f32[128]{0:T(128)}, u32[]{:S(2)}) copy-start(f32[128]{0:T(128)} %param.17) | copy-start | bytes 1540
  81.3 51.8 %all-gather.3.cloned.1.call-start = ((), (), s32[]{:S(2)}) async-start(), calls=%async_computation.3 | async-start | bytes 1310720 | tf_op jit(solution)/shard_map/all_gather | solution.py:100
  83.0 6.1 %collective-permute-start = (bf16[256,128]{1,0:T(8,128)(2,1)S(1)}, bf16[256,128]{1,0:T(8,128)(2,1)S(1)}, u32[]{:S(2)}, u32[]{:S(2)}) collective-permute-start(bf16[256,128]{1,0:T(8,128)(2,1)S(1)} %get-tuple-element.2), channel_id=1, source_target_pairs={{0,4},{4,8},{8,12},{12,0},{1,5},{5,9},{9,13},{13,1},{2,6},{6,10},{... | collective-permute-start | bytes 196616 | tf_op jit(solution)/shard_map/ppermute | solution.py:17
  89.1 6.1 %collective-permute-start.1 = (bf16[256,128]{1,0:T(8,128)(2,1)S(1)}, bf16[256,128]{1,0:T(8,128)(2,1)S(1)}, u32[]{:S(2)}, u32[]{:S(2)}) collective-permute-start(bf16[256,128]{1,0:T(8,128)(2,1)S(1)} %collective-permute-done), channel_id=1, source_target_pairs={{0,4},{4,8},{8,12},{12,0},{1,5},{5,9},{9,13},{13,1},{2,6},{6,10},{... | collective-permute-start | bytes 196616 | tf_op jit(solution)/shard_map/ppermute | solution.py:17
  95.2 14.2 %collective-permute-start.2 = (bf16[256,128]{1,0:T(8,128)(2,1)S(1)}, bf16[256,128]{1,0:T(8,128)(2,1)S(1)}, u32[]{:S(2)}, u32[]{:S(2)}) collective-permute-start(bf16[256,128]{1,0:T(8,128)(2,1)S(1)} %collective-permute-done.1), channel_id=1, source_target_pairs={{0,4},{4,8},{8,12},{12,0},{1,5},{5,9},{9,13},{13,1},{2,6},{6,10},{... | collective-permute-start | bytes 196616 | tf_op jit(solution)/shard_map/ppermute | solution.py:17
  111.0 7.8 %copy-start.3 = (f32[192,2]{0,1:T(2,128)S(1)}, f32[192,2]{0,1:T(2,128)}, u32[]{:S(2)}) copy-start(f32[192,2]{0,1:T(2,128)} %param.23) | copy-start | bytes 4612
  111.0 7.9 %copy-start.6 = (f32[192]{0:T(256)S(1)}, f32[192]{0:T(256)}, u32[]{:S(2)}) copy-start(f32[192]{0:T(256)} %param.22) | copy-start | bytes 2308
  114.2 22.2 %all-to-all-start.1 = ((bf16[4,144,512]{2,1,0:T(8,128)(2,1)}), bf16[4,144,512]{2,1,0:T(8,128)(2,1)S(1)}, u32[]{:S(2)}, u32[]{:S(2)}) async-start(bf16[4,144,512]{2,1,0:T(8,128)(2,1)} %reduce-scatter.2.cloned.1.call-done), calls=%async_computation.2 | async-start | bytes 1179648 | tf_op jit(solution)/shard_map/all_to_all | solution.py:140
Sparse Core Ops, SparseCore 0:
  46.6 23.1 all-gather.4
  81.4 32.7 reduce-scatter.1
  116.3 16.6 all-gather.2
